TPU v7x, 256 devices: a whole 4x4x8 slice. The times are simulated.
256 devices in a mesh: sp: 32 (over z, x), tp: 8 (over y, core).
Axes of the slice: x: 4, y: 4, z: 8, core: 2. Of those that a mesh axis runs over, the one named last changes fastest.
Arguments:
- tokens: bfloat16 [2, 6144, 4096], P(None, 'sp', 'tp'), may hold values from -12 to 12
- query_weight: bfloat16 [4096, 2048], P(None, 'tp'), may hold values from -0.09375 to 0.09375
- key_weight: bfloat16 [4096, 2048], P(None, 'tp'), may hold values from -0.09375 to 0.09375
- value_weight: bfloat16 [4096, 2048], P(None, 'tp'), may hold values from -0.09375 to 0.09375
- gate_weight: bfloat16 [4096, 2048], P(None, 'tp'), may hold values from -0.09375 to 0.09375
- beta_weight: bfloat16 [4096, 16], P(None, 'tp'), may hold values from -0.09375 to 0.09375
- decay_weight: bfloat16 [4096, 16], P(None, 'tp'), may hold values from -0.09375 to 0.09375
- beta_bias: float32 [16], P('tp'), may hold values from -6 to -3
- rate_log: float32 [16], P('tp'), may hold values from -12 to -2.5
- out_gain: float32 [128], replicated, may hold values from 0.1 to 1.9
- new_query: bfloat16 [2, 16, 128], P(None, 'tp'), may hold values from -6 to 6
- new_key: bfloat16 [2, 16, 128], P(None, 'tp'), may hold values from -6 to 6
- new_value: bfloat16 [2, 16, 128], P(None, 'tp'), may hold values from -6 to 6
- new_beta: float32 [2, 16], P(None, 'tp'), may hold values from 0.1 to 0.9
- new_decay: float32 [2, 16], P(None, 'tp'), may hold values from 0.3 to 1
Outputs:
- mixed_out: bfloat16 [2, 6144, 2048], P(None, 'sp', 'tp')
- cache: bfloat16 [2, 16, 128, 128], P(None, 'tp', 'sp')
- first_out: float32 [2, 2048], P(None, 'tp')
All inputs are finite; a program needn't handle non-finite values.
Results may differ from a plain program's by a relative error of at most 0.0073.
Values may be sent and summed in bfloat16 or wider, within the bound.
No kernel may reach another device: no remote copies, remote signals or barrier semaphores. Data moves between devices by JAX's collectives and lax.ppermute only.
A program may use at most 64 MiB of HBM per device.

v0:
```python
import jax
import jax.numpy as jnp
from jax import lax
from jax.sharding import Mesh
from jax.sharding import PartitionSpec as P

BLOCK = 64
SP = ("sp_0", "sp_1")
unit_floor = 1.0
norm_floor = 0.001
highest = lax.Precision.HIGHEST


def neutral_like(value, identity):
    return jax.tree.map(
        lambda a, e: jnp.broadcast_to(jnp.asarray(e, a.dtype), a.shape), value, identity
    )


def carried_in(value, axes, combine, identity):
    before = start = neutral_like(value, identity)
    subtotal = value
    for axis in reversed(axes):
        length, index = (lax.axis_size(axis), lax.axis_index(axis))
        pieces = jax.tree.map(lambda part: lax.all_gather(part, axis), subtotal)
        inside, subtotal = (start, start)
        for k in range(length):
            passed = k < index
            subtotal = combine(subtotal, jax.tree.map(lambda part: part[k], pieces))
            inside = jax.tree.map(lambda new, old: jnp.where(passed, new, old), subtotal, inside)
        before = combine(inside, before)
    return before


def split_up(value, dim, length):
    before, after = (value.shape[:dim], value.shape[dim + 1 :])
    return jnp.moveaxis(value.reshape(*before, length, -1, *after), dim, 0)


def summed_on_arrival(value, axis, dim):
    parts = split_up(value, dim, lax.axis_size(axis))
    arrived = lax.all_to_all(parts, axis, split_axis=0, concat_axis=0, tiled=True)
    return arrived.astype(jnp.float32).sum(axis=0)


def copy_for_each(value, axis):
    length = lax.axis_size(axis)
    return lax.all_to_all(
        jnp.broadcast_to(value[None], (length, *value.shape)), axis, 0, 0, tiled=True
    )


def over_copies(value, axis):
    everything = copy_for_each(value, axis)
    return jnp.sum(everything, axis=0)


def in_one(arrays, axis):
    ravelled, at, gathered = (jnp.concatenate([a.reshape(-1) for a in arrays]), 0, [])
    subtotal = over_copies(ravelled, axis)
    for a in arrays:
        gathered.append(subtotal[at : at + a.size].reshape(a.shape))
        at += a.size
    return tuple(gathered)


def matmul(form, left, right):
    return jnp.einsum(form, left, right, precision=highest)


def unit_rows(values):
    return values * lax.rsqrt(jnp.sum(values * values, axis=-1, keepdims=True) + unit_floor)


def head_norm(values, out_gain):
    return (
        values
        * lax.rsqrt(jnp.mean(values * values, axis=-1, keepdims=True) + norm_floor)
        * out_gain
    )


def stored(values):
    return lax.optimization_barrier(values.astype(jnp.bfloat16)).astype(jnp.float32)


def unit_lower_inverse(lower_part):
    extent = lower_part.shape[-1]
    nilpotent = -lower_part
    inverse = jnp.eye(extent, dtype=jnp.float32) + nilpotent
    for _ in range(extent.bit_length() - 2):
        nilpotent = matmul("...ij,...jk->...ik", nilpotent, nilpotent)
        inverse = inverse + matmul("...ij,...jk->...ik", nilpotent, inverse)
    return inverse


def prepare(
    query_rows,
    key_rows,
    value_rows,
    beta_in,
    decay_in,
    beta_bias,
    rate_log,
    seq_count,
    length,
    head_count,
):
    extent = query_rows.shape[-1] // head_count
    blocks = length // BLOCK

    def by_head(values):
        shaped = values.reshape(seq_count, blocks, BLOCK, head_count, extent)
        return shaped.transpose(0, 3, 1, 2, 4).reshape(
            seq_count * head_count, blocks, BLOCK, extent
        )

    def by_scalar(values):
        shaped = values.reshape(seq_count, blocks, BLOCK, head_count)
        return shaped.transpose(0, 3, 1, 2).reshape(seq_count * head_count, blocks, BLOCK)

    queries = unit_rows(by_head(query_rows))
    key_unit = unit_rows(by_head(key_rows))
    values = by_head(value_rows)
    strength = by_scalar(jax.nn.sigmoid(beta_in + beta_bias))
    decays = by_scalar(-jnp.exp(rate_log) * jax.nn.softplus(decay_in))
    return (queries, key_unit, values, strength, decays)


def block_terms(queries, key_unit, values, strength, decays):
    extent = decays.shape[-1]
    cumulative = jnp.cumsum(decays, axis=-1)
    causal = jnp.tril(jnp.ones((extent, extent), bool))
    strict = jnp.tril(jnp.ones((extent, extent), bool), -1)
    spread = cumulative[..., :, None] - cumulative[..., None, :]
    weights = jnp.where(causal, jnp.exp(jnp.where(causal, spread, 0.0)), 0.0)
    key_beta = key_unit * strength[..., None]
    lower_part = jnp.where(strict, matmul("...td,...sd->...ts", key_beta, key_unit) * weights, 0.0)
    inverse = unit_lower_inverse(lower_part)
    update = matmul("...ts,...se->...te", inverse, values * strength[..., None])
    carry_w = matmul("...ts,...sd->...td", inverse, key_beta * jnp.exp(cumulative)[..., None])
    scores = matmul("...td,...sd->...ts", queries, key_unit) * weights
    query_decay = queries * jnp.exp(cumulative)[..., None]
    last_log = cumulative[..., -1]
    key_decay = key_unit * jnp.exp(last_log[..., None] - cumulative)[..., None]
    return (update, carry_w, query_decay, scores, key_decay, last_log)


def finish_read(recall, retrieve, query_unit, key_unit, new_value, new_beta, new_decay, out_gain):
    seq_count, head_count, extent = recall.shape
    intersect = jnp.sum(key_unit * query_unit, axis=-1)
    fresh_values = new_value.astype(jnp.float32) - new_decay[..., None] * retrieve
    read_heads = new_decay[..., None] * recall + (new_beta * intersect)[..., None] * fresh_values
    return head_norm(read_heads, out_gain).reshape(seq_count, head_count * extent)


def project_rows(shard_rows, weights):
    row_count = shard_rows.shape[-1]
    flat_rows = shard_rows.reshape(-1, row_count)
    return tuple(
        (jnp.dot(flat_rows, weight, preferred_element_type=jnp.float32) for weight in weights)
    )


def shards(
    tokens,
    query_weight,
    key_weight,
    value_weight,
    gate_weight,
    beta_weight,
    decay_weight,
    beta_bias,
    rate_log,
    out_gain,
    new_query,
    new_key,
    new_value,
    new_beta,
    new_decay,
):
    seq_count, span_len, _ = tokens.shape
    head_count = rate_log.shape[0]
    weights = (query_weight, key_weight, value_weight, gate_weight, beta_weight, decay_weight)
    totals = project_rows(lax.all_gather(tokens, "tp", axis=2, tiled=True), weights)
    query_rows = stored(totals[0])
    key_rows = stored(totals[1])
    value_rows = stored(totals[2])
    gate_rows = stored(totals[3])
    prepared = prepare(
        query_rows,
        key_rows,
        value_rows,
        totals[4],
        totals[5],
        beta_bias,
        rate_log,
        seq_count,
        span_len,
        head_count,
    )
    block_data = block_terms(*prepared)
    batch_size = block_data[0].shape[0]
    extent = block_data[0].shape[-1]
    identity = jnp.broadcast_to(jnp.eye(extent, dtype=jnp.float32), (batch_size, extent, extent))

    def advance(carried, inputs):
        state_now, reach_map = carried
        u_block, w_block, qg_block, score_block, kd_block, gl_block = inputs
        fresh_values = u_block - matmul("btd,bde->bte", w_block, state_now)
        block_out = matmul("btd,bde->bte", qg_block, state_now) + matmul(
            "bts,bse->bte", score_block, fresh_values
        )
        reach_rows = qg_block - matmul("bts,bsd->btd", score_block, w_block)
        factor = jnp.exp(gl_block)[:, None, None]
        transit = factor * identity - matmul("bsd,bse->bde", kd_block, w_block)
        state_next = state_now * factor + matmul("bsd,bse->bde", kd_block, fresh_values)
        map_next = matmul("bde,bef->bdf", transit, reach_map)
        return ((state_next, map_next), (block_out, matmul("btd,bde->bte", reach_rows, reach_map)))

    inputs = tuple((jnp.moveaxis(member, 1, 0) for member in block_data))
    start_state = jnp.zeros((batch_size, extent, extent), jnp.float32)
    (local_state, local_map), (local_out, reach_all) = lax.scan(
        advance, (start_state, identity), inputs
    )

    def compose(earlier, later):
        return (
            matmul("bde,bef->bdf", later[0], earlier[0]),
            matmul("bde,bef->bdf", later[0], earlier[1]) + later[1],
        )

    prefix = carried_in(
        (local_map, local_state), SP, compose, (identity, jnp.zeros_like(local_state))
    )
    incoming = prefix[1]
    block_total = local_out + matmul("nbtd,bde->nbte", reach_all, incoming)
    blocks = span_len // BLOCK
    heads_out = block_total.reshape(blocks, seq_count, head_count, BLOCK, extent).transpose(
        1, 0, 3, 2, 4
    )
    heads_out = heads_out.reshape(seq_count, span_len, head_count, extent)
    gate_values = gate_rows.reshape(seq_count, span_len, head_count, extent)
    mixed_out = (head_norm(heads_out, out_gain) * jax.nn.silu(gate_values)).astype(jnp.bfloat16)
    mixed_out = mixed_out.reshape(seq_count, span_len, head_count * extent)
    final_state = matmul("bde,bef->bdf", local_map, incoming) + local_state
    final_cast = final_state.reshape(seq_count, head_count, extent, extent).astype(jnp.bfloat16)
    row_count = extent // lax.axis_size(SP)
    row_start = lax.axis_index(SP) * row_count
    query_unit = unit_rows(new_query.astype(jnp.float32))
    key_unit = unit_rows(new_key.astype(jnp.float32))
    is_last = lax.axis_index(SP) == lax.axis_size(SP) - 1
    own_term = jnp.where(is_last, final_cast.astype(jnp.float32), 0.0)
    cache_rows = summed_on_arrival(own_term.astype(jnp.bfloat16), SP, 2).astype(jnp.bfloat16)
    memory = lax.optimization_barrier(cache_rows).astype(jnp.float32)
    query_part = lax.dynamic_slice_in_dim(query_unit, row_start, row_count, 2)
    key_part = lax.dynamic_slice_in_dim(key_unit, row_start, row_count, 2)
    recall, retrieve = in_one(
        (matmul("shde,shd->she", memory, query_part), matmul("shde,shd->she", memory, key_part)), SP
    )
    first_out = finish_read(
        recall, retrieve, query_unit, key_unit, new_value, new_beta, new_decay, out_gain
    )
    return (mixed_out, cache_rows, first_out)


def solution(mesh):
    torus = Mesh(mesh.devices.reshape(8, 4, mesh.shape["tp"]), ("sp_0", "sp_1", "tp"))
    in_specs = (
        P(None, SP, "tp"),
        P(None, "tp"),
        P(None, "tp"),
        P(None, "tp"),
        P(None, "tp"),
        P(None, "tp"),
        P(None, "tp"),
        P("tp"),
        P("tp"),
        P(),
        P(None, "tp", None),
        P(None, "tp", None),
        P(None, "tp", None),
        P(None, "tp"),
        P(None, "tp"),
    )
    out_specs = (P(None, SP, "tp"), P(None, "tp", SP, None), P(None, "tp"))
    return jax.shard_map(
        shards, mesh=torus, in_specs=in_specs, out_specs=out_specs, check_vma=False
    )
```

profile of v0, /device:TPU:8, one launch (start us, length us, event | category | flops | bytes accessed | tf_op | source)
XLA Modules:
  0.0 295.3 jit_solution(3390538268324986770)
XLA Ops:
  9.4 32.6 %all-gather.10.cloned.1.call-done = bf16[2,192,4096]{2,1,0:T(8,128)(2,1)} async-done(((bf16[2,192,512]{2,1,0:T(8,128)(2,1)}), bf16[2,192,4096]{2,1,0:T(8,128)(2,1)}) %all-gather.10.cloned.1.call-update) | async-done | bytes 3145744 | tf_op jit(solution)/shard_map/all_gather | solution.py:185
  42.0 2.8 fusion.91
  46.8 2.9 convolution_convert_fusion.1
  51.3 2.8 fusion.50
  54.3 3.5 %convolution_convert_fusion.3 = bf16[384,256]{1,0:T(8,128)(2,1)S(1)} fusion(bf16[384,4096]{1,0:T(8,128)(2,1)} %bitcast.236, bf16[4096,256]{1,0:T(8,128)(2,1)} %param.19), kind=kOutput, calls=%fused_computation.61 | convolution fusion | flops 805404672 | bytes 5439488 | tf_op jit(solution)/shard_map/dot_general | solution.py:161
  59.4 3.6 %convolution_convert_fusion.2 = bf16[384,256]{1,0:T(8,128)(2,1)S(1)} fusion(bf16[384,4096]{1,0:T(8,128)(2,1)} %bitcast.237, bf16[4096,256]{1,0:T(8,128)(2,1)} %param.20), kind=kOutput, calls=%fused_computation.60 | convolution fusion | flops 805404672 | bytes 5439488 | tf_op jit(solution)/shard_map/dot_general | solution.py:161
  73.8 1.5 fusion.39
  75.3 29.5 %while.17 = (s32[]{:T(128)}, f32[4,128,128]{2,1,0:T(8,128)S(1)}, f32[4,128,128]{2,1,0:T(8,128)S(1)}, f32[3,4,64,128]{3,2,0,1:T(8,128)}, f32[3,4,64,128]{3,2,0,1:...) while((s32[]{:T(128)}, f32[4,128,128]{2,1,0:T(8,128)S(1)}, ...), condition=%wide.region_4.5_spmd.clone, body=%wide.region_3.4_spmd.clone.sunk | while | flops 403210240 | bytes 5445847 | solution.py:223
  79.5 1.5 convolution_add_fusion.23
  83.2 1.5 convolution_subtract_fusion.7
  89.3 1.5 convolution_add_fusion.23
  99.2 1.5 convolution_add_fusion.23
  106.4 26.9 %all-gather.12.cloned.1.call-done = f32[16,128,128]{2,1,0:T(8,128)} async-done(((f32[4,128,128]{2,1,0:T(8,128)}), f32[16,128,128]{2,1,0:T(8,128)}) %all-gather.12.cloned.1.call-update) | async-done | bytes 1048592 | tf_op jit(solution)/shard_map/all_gather | solution.py:25
  139.8 22.4 %all-gather.16.cloned.1.call-done = f32[16,128,128]{2,1,0:T(8,128)} async-done(((f32[4,128,128]{2,1,0:T(8,128)}), f32[16,128,128]{2,1,0:T(8,128)}) %all-gather.16.cloned.1.call-update) | async-done | bytes 1048592 | tf_op jit(solution)/shard_map/all_gather | solution.py:25
  168.5 4.3 %convolution_convert_fusion = bf16[384,256]{1,0:T(8,128)(2,1)} fusion(bf16[384,4096]{1,0:T(8,128)(2,1)} %bitcast.238, bf16[4096,256]{1,0:T(8,128)(2,1)} %param.21), kind=kOutput, calls=%fused_computation.58 | convolution fusion | flops 805404672 | bytes 5439488 | tf_op jit(solution)/shard_map/dot_general | solution.py:161
  173.9 31.2 %all-gather.14.cloned.1.call-done = f32[32,128,128]{2,1,0:T(8,128)} async-done(((f32[4,128,128]{2,1,0:T(8,128)}), f32[32,128,128]{2,1,0:T(8,128)}) %all-gather.14.cloned.1.call-update) | async-done | bytes 2097168 | tf_op jit(solution)/shard_map/all_gather | solution.py:25
  205.1 41.1 %all-gather.18.cloned.1.call-done = f32[32,128,128]{2,1,0:T(8,128)} async-done(((f32[4,128,128]{2,1,0:T(8,128)}), f32[32,128,128]{2,1,0:T(8,128)}) %all-gather.18.cloned.1.call-update) | async-done | bytes 2097168 | tf_op jit(solution)/shard_map/all_gather | solution.py:25
  246.2 1.5 convolution_add_fusion.20
  254.7 7.1 %all-to-all-start = ((bf16[32,2,2,4,128]{4,3,2,1,0:T(4,128)(2,1)}), bf16[32,2,2,4,128]{4,3,2,1,0:T(4,128)(2,1)S(1)}, u32[]{:S(2)}, u32[]{:S(2)}) async-start(bf16[32,2,2,4,128]{4,3,2,1,0:T(4,128)(2,1)} %bitcast.193), calls=%async_computation | async-start | bytes 262144 | tf_op jit(solution)/shard_map/all_to_all | solution.py:42
  261.8 1.6 fusion.38
  265.2 7.1 %all-to-all-done = bf16[32,2,2,4,128]{4,3,2,1,0:T(4,128)(2,1)S(1)} async-done(((bf16[32,2,2,4,128]{4,3,2,1,0:T(4,128)(2,1)}), bf16[32,2,2,4,128]{4,3,2,1,0:T(4,128)(2,1)S(1)}, u32[]{:S(2)}, u32[]{:S(2)}) %all-to-all-start) | async-done | bytes 131104 | tf_op jit(solution)/shard_map/all_to_all | solution.py:42
  273.4 3.8 %all-to-all-start.1 = ((f32[32,1,1024]{2,1,0:T(1,128)}), f32[32,1,1024]{2,1,0:T(1,128)S(1)}, u32[]{:S(2)}, u32[]{:S(2)}) async-start(f32[32,1,1024]{2,1,0:T(1,128)} %broadcast_in_dim.80), calls=%async_computation.1 | async-start | bytes 262144 | tf_op jit(solution)/shard_map/all_to_all | solution.py:48
  277.3 1.7 fusion.60
  279.0 8.8 %all-to-all-done.1 = f32[32,1,1024]{2,1,0:T(1,128)S(1)} async-done(((f32[32,1,1024]{2,1,0:T(1,128)}), f32[32,1,1024]{2,1,0:T(1,128)S(1)}, u32[]{:S(2)}, u32[]{:S(2)}) %all-to-all-start.1) | async-done | bytes 131104 | tf_op jit(solution)/shard_map/all_to_all | solution.py:48
  (195 shorter events, 67.1 us)
Async XLA Ops:
  7.2 39.7 %copy-start = (bf16[4096,256]{1,0:T(8,128)(2,1)S(1)}, bf16[4096,256]{1,0:T(8,128)(2,1)}, u32[]{:S(2)}) copy-start(bf16[4096,256]{1,0:T(8,128)(2,1)} %param.18) | copy-start | bytes 6291460
  7.2 34.8 %all-gather.10.cloned.1.call-start = ((), (), s32[]{:S(2)}) async-start(), calls=%async_computation.2 | async-start | bytes 3538944 | tf_op jit(solution)/shard_map/all_gather | solution.py:185
  7.9 125.4 %all-gather.12.cloned.1.call-start = ((), (), s32[]{:S(2)}) async-start(), calls=%async_computation.3 | async-start | bytes 1310720 | tf_op jit(solution)/shard_map/all_gather | solution.py:25
  59.4 3.8 %copy-start.20 = (f32[2,2,3,64,128]{4,3,1,0,2:T(8,128)S(1)}, f32[2,2,3,64,128]{4,3,1,0,2:T(8,128)}, u32[]{:S(2)}) copy-start(f32[2,2,3,64,128]{4,3,1,0,2:T(8,128)} %copy.189) | copy-start | bytes 1179652
  105.6 56.6 %all-gather.16.cloned.1.call-start = ((), (), s32[]{:S(2)}) async-start(), calls=%async_computation.5 | async-start | bytes 1310720 | tf_op jit(solution)/shard_map/all_gather | solution.py:25
  106.3 98.8 %all-gather.14.cloned.1.call-start = ((), (), s32[]{:S(2)}) async-start(), calls=%async_computation.4 | async-start | bytes 2359296 | tf_op jit(solution)/shard_map/all_gather | solution.py:25
  133.3 4.2 %copy-start.3 = (f32[16,128,128]{2,1,0:T(8,128)S(1)}, f32[16,128,128]{2,1,0:T(8,128)}, u32[]{:S(2)}) copy-start(f32[16,128,128]{2,1,0:T(8,128)} %all-gather.12.cloned.1.call-done) | copy-start | bytes 3145732
  139.7 106.4 %all-gather.18.cloned.1.call-start = ((), (), s32[]{:S(2)}) async-start(), calls=%async_computation.6 | async-start | bytes 2359296 | tf_op jit(solution)/shard_map/all_gather | solution.py:25
  162.2 3.5 %copy-start.22 = (f32[16,128,128]{2,1,0:T(8,128)S(1)}, f32[16,128,128]{2,1,0:T(8,128)}, u32[]{:S(2)}) copy-start(f32[16,128,128]{2,1,0:T(8,128)} %all-gather.16.cloned.1.call-done) | copy-start | bytes 3145732
  163.6 4.4 %copy-start.26 = (bf16[2,2,128]{2,1,0:T(2,128)(2,1)S(1)}, bf16[2,2,128]{2,1,0:T(2,128)(2,1)}, u32[]{:S(2)}) copy-start(bf16[2,2,128]{2,1,0:T(2,128)(2,1)} %param.27) | copy-start | bytes 3076
  163.6 4.5 %copy-start.27 = (bf16[2,2,128]{2,1,0:T(2,128)(2,1)S(1)}, bf16[2,2,128]{2,1,0:T(2,128)(2,1)}, u32[]{:S(2)}) copy-start(bf16[2,2,128]{2,1,0:T(2,128)(2,1)} %param.28) | copy-start | bytes 3076
  163.6 4.7 %copy-start.29 = (f32[2,2]{1,0:T(2,128)S(1)}, f32[2,2]{1,0:T(2,128)}, u32[]{:S(2)}) copy-start(f32[2,2]{1,0:T(2,128)} %param.30) | copy-start | bytes 52
  163.6 4.8 %copy-start.32 = (f32[128]{0:T(128)S(1)}, f32[128]{0:T(128)}, u32[]{:S(2)}) copy-start(f32[128]{0:T(128)} %param.26) | copy-start | bytes 1540
  168.4 4.3 %copy-start.8 = (f32[4,128,128]{2,1,0:T(8,128)S(1)}, f32[4,128,128]{2,1,0:T(8,128)}, u32[]{:S(2)}) copy-start(f32[4,128,128]{2,1,0:T(8,128)} %copy-done.7) | copy-start | bytes 786436
  168.4 4.3 %copy-start.10 = (f32[4,128,128]{2,1,0:T(8,128)S(1)}, f32[4,128,128]{2,1,0:T(8,128)}, u32[]{:S(2)}) copy-start(f32[4,128,128]{2,1,0:T(8,128)} %copy-done.9) | copy-start | bytes 786436
  168.4 4.3 %copy-start.12 = (f32[4,128,128]{2,1,0:T(8,128)S(1)}, f32[4,128,128]{2,1,0:T(8,128)}, u32[]{:S(2)}) copy-start(f32[4,128,128]{2,1,0:T(8,128)} %fusion.109) | copy-start | bytes 786436
  168.4 4.3 %copy-start.18 = (f32[4,128,128]{2,1,0:T(8,128)S(1)}, f32[4,128,128]{2,1,0:T(8,128)}, u32[]{:S(2)}) copy-start(f32[4,128,128]{2,1,0:T(8,128)} %copy-done.17) | copy-start | bytes 786436
  246.2 3.0 %copy-start.6 = (f32[32,128,128]{2,1,0:T(8,128)S(1)}, f32[32,128,128]{2,1,0:T(8,128)}, u32[]{:S(2)}) copy-start(f32[32,128,128]{2,1,0:T(8,128)} %all-gather.14.cloned.1.call-done) | copy-start | bytes 6291460
  246.2 4.3 %copy-start.19 = (f32[32,128,128]{2,1,0:T(8,128)S(1)}, f32[32,128,128]{2,1,0:T(8,128)}, u32[]{:S(2)}) copy-start(f32[32,128,128]{2,1,0:T(8,128)} %all-gather.18.cloned.1.call-done) | copy-start | bytes 6291460
  254.7 17.6 %all-to-all-start = ((bf16[32,2,2,4,128]{4,3,2,1,0:T(4,128)(2,1)}), bf16[32,2,2,4,128]{4,3,2,1,0:T(4,128)(2,1)S(1)}, u32[]{:S(2)}, u32[]{:S(2)}) async-start(bf16[32,2,2,4,128]{4,3,2,1,0:T(4,128)(2,1)} %bitcast.193), calls=%async_computation | async-start | bytes 262144 | tf_op jit(solution)/shard_map/all_to_all | solution.py:42
  263.9 24.0 %copy-start.30 = (bf16[2,2,128]{2,1,0:T(2,128)(2,1)S(1)}, bf16[2,2,128]{2,1,0:T(2,128)(2,1)}, u32[]{:S(2)}) copy-start(bf16[2,2,128]{2,1,0:T(2,128)(2,1)} %param.29) | copy-start | bytes 3076
  263.9 24.0 %copy-start.31 = (f32[2,2]{1,0:T(2,128)S(1)}, f32[2,2]{1,0:T(2,128)}, u32[]{:S(2)}) copy-start(f32[2,2]{1,0:T(2,128)} %param.31) | copy-start | bytes 52
  272.4 16.4 %copy-start.25 = (bf16[2,2,4,128]{3,2,1,0:T(4,128)(2,1)}, bf16[2,2,4,128]{3,2,1,0:T(4,128)(2,1)S(1)}, u32[]{:S(2)}) copy-start(bf16[2,2,4,128]{3,2,1,0:T(4,128)(2,1)S(1)} %reduce_sum.87) | copy-start | bytes 12292
  273.4 14.4 %all-to-all-start.1 = ((f32[32,1,1024]{2,1,0:T(1,128)}), f32[32,1,1024]{2,1,0:T(1,128)S(1)}, u32[]{:S(2)}, u32[]{:S(2)}) async-start(f32[32,1,1024]{2,1,0:T(1,128)} %broadcast_in_dim.80), calls=%async_computation.1 | async-start | bytes 262144 | tf_op jit(solution)/shard_map/all_to_all | solution.py:48
  (16 other events, 17.8 us)
Sparse Core Ops, SparseCore 0:
  9.8 32.1 all-gather.9
  105.7 27.5 all-gather.11
  135.1 27.0 all-gather.15
  163.8 41.2 all-gather.13
  206.7 39.4 all-gather.17
where the time goes:
time: 296 us; the launch traced here: 295 us
  waiting for transfers between devices  172 us (58%)
  matrix products  75.5 us (26%)
  between operations  14.6 us (5%)
  local copies, waits for them, and re-layouts  13.8 us (5%)
  starting transfers between devices  11.1 us (4%)
  other arithmetic  8.51 us (3%)
    all_gather x4, waiting for transfers between devices, carried_in(): pieces = jax.tree.map(lambda part: lax.all_gather(part, axis), subtotal)  122 us
    dot_general x61, matrix products, matmul(): return jnp.einsum(form, left, right, precision=highest)  55.6 us
    all_gather x1, waiting for transfers between devices, shards(): lax.all_gather(tokens, 'tp', axis=2, tiled=True)  32.6 us
    dot_general x6, matrix products, project_rows(): jnp.dot(flat_rows, weight, preferred_element_type=jnp.float32)  19.9 us
    all_to_all x1, waiting for transfers between devices, copy_for_each(): lax.all_to_all(jnp.broadcast_to(value[None], (length, *value.shape)), axi...  8.81 us
    all_to_all x1, waiting for transfers between devices, summed_on_arrival(): lax.all_to_all(parts, axis, split_axis=0, concat_axis=0, tiled=True)  7.1 us
    all_to_all x1, starting transfers between devices, summed_on_arrival(): lax.all_to_all(parts, axis, split_axis=0, concat_axis=0, tiled=True)  7.08 us
  transfers between devices with their start and end apart: 7, of which 7 were waited for; matrix products, arithmetic and copies ran while one was open for 7% of the time, Pallas kernels for 0%

commit v1 on v0

--- a/solution.py
+++ b/solution.py
@@ -9,6 +9,12 @@
 unit_floor = 1.0
 norm_floor = 0.001
 highest = lax.Precision.HIGHEST
+
+
+def tiled_gather(x, axis, dim):
+    length = lax.axis_size(axis)
+    repeats = [length if d == dim else 1 for d in range(x.ndim)]
+    return lax.all_to_all(jnp.tile(x, repeats), axis, split_axis=dim, concat_axis=dim, tiled=True)
 
 
 def neutral_like(value, identity):
@@ -182,7 +188,7 @@
     seq_count, span_len, _ = tokens.shape
     head_count = rate_log.shape[0]
     weights = (query_weight, key_weight, value_weight, gate_weight, beta_weight, decay_weight)
-    totals = project_rows(lax.all_gather(tokens, "tp", axis=2, tiled=True), weights)
+    totals = project_rows(tiled_gather(tokens, "tp", 2), weights)
     query_rows = stored(totals[0])
     key_rows = stored(totals[1])
     value_rows = stored(totals[2])

time: 296 us -> 334 us (1.13)
  local copies, waits for them, and re-layouts: 13.8 us -> 28.9 us
  waiting for transfers between devices: 172 us -> 186 us
  starting transfers between devices: 11.1 us -> 17.8 us
    all_to_all x0 -> x1, waiting for transfers between devices: none -> 48.2 us  [tiled_gather(): lax.all_to_all(jnp.tile(x, repeats), axis, split_axis=dim, concat_axis=di...]
    all_gather x1 -> x0, waiting for transfers between devices: 32.6 us -> none  [shards(): lax.all_gather(tokens, 'tp', axis=2, tiled=True)]
    all_to_all x0 -> x1, local copies, waits for them, and re-layouts: none -> 11 us  [tiled_gather(): lax.all_to_all(jnp.tile(x, repeats), axis, split_axis=dim, concat_axis=di...]
    all_to_all x0 -> x1, starting transfers between devices: none -> 6.74 us  [tiled_gather(): lax.all_to_all(jnp.tile(x, repeats), axis, split_axis=dim, concat_axis=di...]
    another operation x0 -> x1, local copies, waits for them, and re-layouts: none -> 4.18 us  [tiled_gather(): jnp.tile(x, repeats)]
    unnamed x68 -> x71, local copies, waits for them, and re-layouts: 5.89 us -> 6.79 us
  transfers between devices with their start and end apart: 7 -> 7, of which waited for: 7 -> 7; matrix products, arithmetic and copies ran while one was open for 7% -> 6% of each run, Pallas kernels for 0% -> 0%
where the time goes in v1:
time: 334 us; the launch traced here: 333 us
  waiting for transfers between devices  186 us (56%)
  matrix products  78.5 us (24%)
  local copies, waits for them, and re-layouts  28.9 us (9%)
  starting transfers between devices  17.8 us (5%)
  between operations  14.6 us (4%)
  other arithmetic  7.13 us (2%)
    all_gather x4, waiting for transfers between devices, carried_in(): pieces = jax.tree.map(lambda part: lax.all_gather(part, axis), subtotal)  121 us
    dot_general x61, matrix products, matmul(): return jnp.einsum(form, left, right, precision=highest)  58.6 us
    all_to_all x1, waiting for transfers between devices, tiled_gather(): lax.all_to_all(jnp.tile(x, repeats), axis, split_axis=dim, concat_axis=di...  48.2 us
    dot_general x6, matrix products, project_rows(): jnp.dot(flat_rows, weight, preferred_element_type=jnp.float32)  19.9 us
    all_to_all x1, local copies, waits for them, and re-layouts, tiled_gather(): lax.all_to_all(jnp.tile(x, repeats), axis, split_axis=dim, concat_axis=di...  11 us
    all_to_all x1, waiting for transfers between devices, copy_for_each(): lax.all_to_all(jnp.broadcast_to(value[None], (length, *value.shape)), axi...  8.81 us
    all_to_all x1, waiting for transfers between devices, summed_on_arrival(): lax.all_to_all(parts, axis, split_axis=0, concat_axis=0, tiled=True)  7.1 us
    all_to_all x1, starting transfers between devices, summed_on_arrival(): lax.all_to_all(parts, axis, split_axis=0, concat_axis=0, tiled=True)  7.08 us
  transfers between devices with their start and end apart: 7, of which 7 were waited for; matrix products, arithmetic and copies ran while one was open for 6% of the time, Pallas kernels for 0%

profile of v1, /device:TPU:8, one launch (start us, length us, event | category | flops | bytes accessed | tf_op | source)
XLA Modules:
  0.0 332.8 jit_solution(17022759519218053495)
XLA Ops:
  8.7 4.2 %tile.4 = bf16[2,192,8,512]{1,0,3,2:T(2,128)(2,1)} broadcast(bf16[2,192,512]{1,0,2:T(2,128)(2,1)S(1)} %copy.183), dimensions={0,1,3} | broadcast | bytes 3538944 | tf_op jit(solution)/shard_map/tile | solution.py:17
  12.8 6.7 %all-to-all-start = ((bf16[2,192,4096]{1,0,2:T(2,128)(2,1)}), bf16[2,192,4096]{1,0,2:T(2,128)(2,1)}, u32[]{:S(2)}, u32[]{:S(2)}) async-start(bf16[2,192,4096]{1,0,2:T(2,128)(2,1)} %bitcast.240), calls=%async_computation | async-start | bytes 8388608 | tf_op jit(solution)/shard_map/all_to_all | solution.py:17
  19.7 48.2 %all-to-all-done = bf16[2,192,4096]{1,0,2:T(2,128)(2,1)} async-done(((bf16[2,192,4096]{1,0,2:T(2,128)(2,1)}), bf16[2,192,4096]{1,0,2:T(2,128)(2,1)}, u32[]{:S(2)}, u32[]{:S(2)}) %all-to-all-start) | async-done | bytes 3145760 | tf_op jit(solution)/shard_map/all_to_all | solution.py:17
  67.9 11.0 %copy.184 = bf16[2,192,4096]{2,1,0:T(8,128)(2,1)} copy(bf16[2,192,4096]{1,0,2:T(2,128)(2,1)} %all-to-all-done) | data formatting | bytes 6291456 | tf_op jit(solution)/shard_map/all_to_all | solution.py:17
  78.9 2.8 fusion.91
  83.3 2.9 convolution_convert_fusion.1
  87.1 2.8 fusion.50
  90.0 3.5 %convolution_convert_fusion.3 = bf16[384,256]{1,0:T(8,128)(2,1)S(1)} fusion(bf16[384,4096]{1,0:T(8,128)(2,1)} %bitcast.237, bf16[4096,256]{1,0:T(8,128)(2,1)} %param.19), kind=kOutput, calls=%fused_computation.61 | convolution fusion | flops 805404672 | bytes 5439488 | tf_op jit(solution)/shard_map/dot_general | solution.py:167
  95.1 3.6 %convolution_convert_fusion.2 = bf16[384,256]{1,0:T(8,128)(2,1)S(1)} fusion(bf16[384,4096]{1,0:T(8,128)(2,1)} %bitcast.238, bf16[4096,256]{1,0:T(8,128)(2,1)} %param.20), kind=kOutput, calls=%fused_computation.60 | convolution fusion | flops 805404672 | bytes 5439488 | tf_op jit(solution)/shard_map/dot_general | solution.py:167
  112.6 30.4 %while.17 = (s32[]{:T(128)}, f32[4,128,128]{2,1,0:T(8,128)S(1)}, f32[4,128,128]{2,1,0:T(8,128)S(1)}, f32[3,4,64,128]{3,2,0,1:T(8,128)}, f32[3,4,64,128]{3,2,0,1:...) while((s32[]{:T(128)}, f32[4,128,128]{2,1,0:T(8,128)S(1)}, ...), condition=%wide.region_4.5_spmd.clone, body=%wide.region_3.4_spmd.clone.sunk | while | flops 403210240 | bytes 5445847 | solution.py:229
  115.1 1.9 fusion.227
  125.2 1.9 fusion.227
  135.3 1.9 fusion.227
  144.5 26.1 %all-gather.9.cloned.1.call-done = f32[16,128,128]{2,1,0:T(8,128)} async-done(((f32[4,128,128]{2,1,0:T(8,128)}), f32[16,128,128]{2,1,0:T(8,128)}) %all-gather.9.cloned.1.call-update) | async-done | bytes 1048592 | tf_op jit(solution)/shard_map/all_gather | solution.py:31
  177.1 22.4 %all-gather.13.cloned.1.call-done = f32[16,128,128]{2,1,0:T(8,128)} async-done(((f32[4,128,128]{2,1,0:T(8,128)}), f32[16,128,128]{2,1,0:T(8,128)}) %all-gather.13.cloned.1.call-update) | async-done | bytes 1048592 | tf_op jit(solution)/shard_map/all_gather | solution.py:31
  205.8 4.3 %convolution_convert_fusion = bf16[384,256]{1,0:T(8,128)(2,1)} fusion(bf16[384,4096]{1,0:T(8,128)(2,1)} %bitcast.239, bf16[4096,256]{1,0:T(8,128)(2,1)} %param.21), kind=kOutput, calls=%fused_computation.58 | convolution fusion | flops 805404672 | bytes 5439488 | tf_op jit(solution)/shard_map/dot_general | solution.py:167
  211.2 31.3 %all-gather.11.cloned.1.call-done = f32[32,128,128]{2,1,0:T(8,128)} async-done(((f32[4,128,128]{2,1,0:T(8,128)}), f32[32,128,128]{2,1,0:T(8,128)}) %all-gather.11.cloned.1.call-update) | async-done | bytes 2097168 | tf_op jit(solution)/shard_map/all_gather | solution.py:31
  242.5 41.1 %all-gather.15.cloned.1.call-done = f32[32,128,128]{2,1,0:T(8,128)} async-done(((f32[4,128,128]{2,1,0:T(8,128)}), f32[32,128,128]{2,1,0:T(8,128)}) %all-gather.15.cloned.1.call-update) | async-done | bytes 2097168 | tf_op jit(solution)/shard_map/all_gather | solution.py:31
  292.2 7.1 %all-to-all-start.1 = ((bf16[32,2,2,4,128]{4,3,2,1,0:T(4,128)(2,1)}), bf16[32,2,2,4,128]{4,3,2,1,0:T(4,128)(2,1)S(1)}, u32[]{:S(2)}, u32[]{:S(2)}) async-start(bf16[32,2,2,4,128]{4,3,2,1,0:T(4,128)(2,1)} %bitcast.194), calls=%async_computation.1 | async-start | bytes 262144 | tf_op jit(solution)/shard_map/all_to_all | solution.py:48
  299.3 1.6 fusion.38
  302.7 7.1 %all-to-all-done.1 = bf16[32,2,2,4,128]{4,3,2,1,0:T(4,128)(2,1)S(1)} async-done(((bf16[32,2,2,4,128]{4,3,2,1,0:T(4,128)(2,1)}), bf16[32,2,2,4,128]{4,3,2,1,0:T(4,128)(2,1)S(1)}, u32[]{:S(2)}, u32[]{:S(2)}) %all-to-all-start.1) | async-done | bytes 131104 | tf_op jit(solution)/shard_map/all_to_all | solution.py:48
  310.9 3.8 %all-to-all-start.2 = ((f32[32,1,1024]{2,1,0:T(1,128)}), f32[32,1,1024]{2,1,0:T(1,128)S(1)}, u32[]{:S(2)}, u32[]{:S(2)}) async-start(f32[32,1,1024]{2,1,0:T(1,128)} %broadcast_in_dim.80), calls=%async_computation.2 | async-start | bytes 262144 | tf_op jit(solution)/shard_map/all_to_all | solution.py:54
  314.7 1.7 fusion.60
  316.5 8.8 %all-to-all-done.2 = f32[32,1,1024]{2,1,0:T(1,128)S(1)} async-done(((f32[32,1,1024]{2,1,0:T(1,128)}), f32[32,1,1024]{2,1,0:T(1,128)S(1)}, u32[]{:S(2)}, u32[]{:S(2)}) %all-to-all-start.2) | async-done | bytes 131104 | tf_op jit(solution)/shard_map/all_to_all | solution.py:54
  (199 shorter events, 71.2 us)
Async XLA Ops:
  7.2 76.1 %copy-start = (bf16[4096,256]{1,0:T(8,128)(2,1)S(1)}, bf16[4096,256]{1,0:T(8,128)(2,1)}, u32[]{:S(2)}) copy-start(bf16[4096,256]{1,0:T(8,128)(2,1)} %param.18) | copy-start | bytes 6291460
  12.8 6.8 %copy-start.33 = (f32[2]{0:T(128)S(1)}, f32[2]{0:T(128)}, u32[]{:S(2)}) copy-start(f32[2]{0:T(128)} %param.25) | copy-start | bytes 28
  12.8 55.1 %all-to-all-start = ((bf16[2,192,4096]{1,0,2:T(2,128)(2,1)}), bf16[2,192,4096]{1,0,2:T(2,128)(2,1)}, u32[]{:S(2)}, u32[]{:S(2)}) async-start(bf16[2,192,4096]{1,0,2:T(2,128)(2,1)} %bitcast.240), calls=%async_computation | async-start | bytes 8388608 | tf_op jit(solution)/shard_map/all_to_all | solution.py:17
  19.6 151.0 %all-gather.9.cloned.1.call-start = ((), (), s32[]{:S(2)}) async-start(), calls=%async_computation.3 | async-start | bytes 1310720 | tf_op jit(solution)/shard_map/all_gather | solution.py:31
  19.7 59.2 %copy-start.23 = (bf16[4096,2]{0,1:T(2,128)(2,1)S(1)}, bf16[4096,2]{0,1:T(2,128)(2,1)}, u32[]{:S(2)}) copy-start(bf16[4096,2]{0,1:T(2,128)(2,1)} %param.23) | copy-start | bytes 49156
  95.1 5.6 %copy-start.20 = (f32[2,2,3,64,128]{4,3,1,0,2:T(8,128)S(1)}, f32[2,2,3,64,128]{4,3,1,0,2:T(8,128)}, u32[]{:S(2)}) copy-start(f32[2,2,3,64,128]{4,3,1,0,2:T(8,128)} %copy.187) | copy-start | bytes 1179652
  143.7 55.8 %all-gather.13.cloned.1.call-start = ((), (), s32[]{:S(2)}) async-start(), calls=%async_computation.5 | async-start | bytes 1310720 | tf_op jit(solution)/shard_map/all_gather | solution.py:31
  144.4 98.1 %all-gather.11.cloned.1.call-start = ((), (), s32[]{:S(2)}) async-start(), calls=%async_computation.4 | async-start | bytes 2359296 | tf_op jit(solution)/shard_map/all_gather | solution.py:31
  170.6 4.2 %copy-start.3 = (f32[16,128,128]{2,1,0:T(8,128)S(1)}, f32[16,128,128]{2,1,0:T(8,128)}, u32[]{:S(2)}) copy-start(f32[16,128,128]{2,1,0:T(8,128)} %all-gather.9.cloned.1.call-done) | copy-start | bytes 3145732
  177.1 106.6 %all-gather.15.cloned.1.call-start = ((), (), s32[]{:S(2)}) async-start(), calls=%async_computation.6 | async-start | bytes 2359296 | tf_op jit(solution)/shard_map/all_gather | solution.py:31
  200.9 4.4 %copy-start.26 = (bf16[2,2,128]{2,1,0:T(2,128)(2,1)S(1)}, bf16[2,2,128]{2,1,0:T(2,128)(2,1)}, u32[]{:S(2)}) copy-start(bf16[2,2,128]{2,1,0:T(2,128)(2,1)} %param.27) | copy-start | bytes 3076
  200.9 4.5 %copy-start.27 = (bf16[2,2,128]{2,1,0:T(2,128)(2,1)S(1)}, bf16[2,2,128]{2,1,0:T(2,128)(2,1)}, u32[]{:S(2)}) copy-start(bf16[2,2,128]{2,1,0:T(2,128)(2,1)} %param.28) | copy-start | bytes 3076
  200.9 4.8 %copy-start.29 = (f32[2,2]{1,0:T(2,128)S(1)}, f32[2,2]{1,0:T(2,128)}, u32[]{:S(2)}) copy-start(f32[2,2]{1,0:T(2,128)} %param.30) | copy-start | bytes 52
  200.9 4.8 %copy-start.32 = (f32[128]{0:T(128)S(1)}, f32[128]{0:T(128)}, u32[]{:S(2)}) copy-start(f32[128]{0:T(128)} %param.26) | copy-start | bytes 1540
  205.7 4.3 %copy-start.8 = (f32[4,128,128]{2,1,0:T(8,128)S(1)}, f32[4,128,128]{2,1,0:T(8,128)}, u32[]{:S(2)}) copy-start(f32[4,128,128]{2,1,0:T(8,128)} %copy-done.7) | copy-start | bytes 786436
  205.8 4.3 %copy-start.10 = (f32[4,128,128]{2,1,0:T(8,128)S(1)}, f32[4,128,128]{2,1,0:T(8,128)}, u32[]{:S(2)}) copy-start(f32[4,128,128]{2,1,0:T(8,128)} %copy-done.9) | copy-start | bytes 786436
  205.8 4.3 %copy-start.12 = (f32[4,128,128]{2,1,0:T(8,128)S(1)}, f32[4,128,128]{2,1,0:T(8,128)}, u32[]{:S(2)}) copy-start(f32[4,128,128]{2,1,0:T(8,128)} %fusion.109) | copy-start | bytes 786436
  205.8 4.3 %copy-start.18 = (f32[4,128,128]{2,1,0:T(8,128)S(1)}, f32[4,128,128]{2,1,0:T(8,128)}, u32[]{:S(2)}) copy-start(f32[4,128,128]{2,1,0:T(8,128)} %copy-done.17) | copy-start | bytes 786436
  283.6 4.3 %copy-start.19 = (f32[32,128,128]{2,1,0:T(8,128)S(1)}, f32[32,128,128]{2,1,0:T(8,128)}, u32[]{:S(2)}) copy-start(f32[32,128,128]{2,1,0:T(8,128)} %all-gather.15.cloned.1.call-done) | copy-start | bytes 6291460
  292.2 17.6 %all-to-all-start.1 = ((bf16[32,2,2,4,128]{4,3,2,1,0:T(4,128)(2,1)}), bf16[32,2,2,4,128]{4,3,2,1,0:T(4,128)(2,1)S(1)}, u32[]{:S(2)}, u32[]{:S(2)}) async-start(bf16[32,2,2,4,128]{4,3,2,1,0:T(4,128)(2,1)} %bitcast.194), calls=%async_computation.1 | async-start | bytes 262144 | tf_op jit(solution)/shard_map/all_to_all | solution.py:48
  301.4 24.0 %copy-start.30 = (bf16[2,2,128]{2,1,0:T(2,128)(2,1)S(1)}, bf16[2,2,128]{2,1,0:T(2,128)(2,1)}, u32[]{:S(2)}) copy-start(bf16[2,2,128]{2,1,0:T(2,128)(2,1)} %param.29) | copy-start | bytes 3076
  301.4 24.0 %copy-start.31 = (f32[2,2]{1,0:T(2,128)S(1)}, f32[2,2]{1,0:T(2,128)}, u32[]{:S(2)}) copy-start(f32[2,2]{1,0:T(2,128)} %param.31) | copy-start | bytes 52
  309.9 16.4 %copy-start.25 = (bf16[2,2,4,128]{3,2,1,0:T(4,128)(2,1)}, bf16[2,2,4,128]{3,2,1,0:T(4,128)(2,1)S(1)}, u32[]{:S(2)}) copy-start(bf16[2,2,4,128]{3,2,1,0:T(4,128)(2,1)S(1)} %reduce_sum.87) | copy-start | bytes 12292
  310.9 14.4 %all-to-all-start.2 = ((f32[32,1,1024]{2,1,0:T(1,128)}), f32[32,1,1024]{2,1,0:T(1,128)S(1)}, u32[]{:S(2)}, u32[]{:S(2)}) async-start(f32[32,1,1024]{2,1,0:T(1,128)} %broadcast_in_dim.80), calls=%async_computation.2 | async-start | bytes 262144 | tf_op jit(solution)/shard_map/all_to_all | solution.py:54
  (17 other events, 20.4 us)
Sparse Core Ops, SparseCore 0:
  143.8 26.7 all-gather.8
  172.4 27.0 all-gather.12
  201.3 41.2 all-gather.10
  244.2 39.4 all-gather.14
